TPU v7x, 32 devices: a whole 2x2x4 slice. The times are simulated.
32 devices in a mesh: sp: 8 (over z, y), tp: 4 (over x, core).
Axes of the slice: x: 2, y: 2, z: 4, core: 2. Of those that a mesh axis runs over, the one named last changes fastest.
Arguments:
- hidden_states: bfloat16 [2048, 4096], P('sp', 'tp'), may hold values from -6 to 6
- norm_gain: float32 [4096], replicated, may hold values from 0.1 to 1.9
- query_weight: bfloat16 [4096, 2048], P('sp', 'tp'), may hold values from -0.09375 to 0.09375
- key_weight: bfloat16 [4096, 2048], P('sp', 'tp'), may hold values from -0.09375 to 0.09375
- value_weight: bfloat16 [4096, 2048], P('sp', 'tp'), may hold values from -0.09375 to 0.09375
- output_gate_weight: bfloat16 [4096, 2048], P('sp', 'tp'), may hold values from -0.09375 to 0.09375
- unit_input_weight: bfloat16 [4096, 2048], P('sp', 'tp'), may hold values from -0.09375 to 0.09375
- unit_gate_weight: bfloat16 [4096, 2048], P('sp', 'tp'), may hold values from -0.09375 to 0.09375
- decay_forward: float32 [16], P('tp'), may hold values from 0 to 16
- decay_backward: float32 [16], P('tp'), may hold values from 0 to 16
- group_gain: float32 [2048], P('tp'), may hold values from 0.1 to 1.9
- group_bias: float32 [2048], P('tp'), may hold values from -3 to 3
- depth_kernel: float32 [31, 2048], P(None, 'tp'), may hold values from -7 to 7
- depth_bias: float32 [2048], P('tp'), may hold values from -3 to 3
- channel_gain: float32 [2048], P('tp'), may hold values from 0.1 to 1.9
- channel_bias: float32 [2048], P('tp'), may hold values from -3 to 3
- retention_out_weight: bfloat16 [2048, 4096], P('tp', 'sp'), may hold values from -0.09375 to 0.09375
- convolution_out_weight: bfloat16 [2048, 4096], P('tp', 'sp'), may hold values from -0.09375 to 0.09375
Outputs:
- mixed_out: bfloat16 [2048, 4096], P(('sp', 'tp'))
All inputs are finite; a program needn't handle non-finite values.
Results may differ from a plain program's by a relative error of at most 0.018.
Values may be sent and summed in bfloat16 or wider, within the bound.
A program may use at most 128 MiB of HBM per device.

v0:
```python
import jax
import jax.numpy as jnp
from jax import lax
from jax.sharding import PartitionSpec as P

HEAD_DIM = 128
CONV_WIDTH = 2048
KERNEL = 31
BLOCK = 128
EPS = 1e-06
THETA = 10000.0


def with_halo(cells, sides, width):
    for axis, dim in sides:
        count = lax.axis_size(axis)
        ends = count - 1
        head = lax.slice_in_dim(cells, 0, width, axis=dim)
        tail = lax.slice_in_dim(cells, cells.shape[dim] - width, cells.shape[dim], axis=dim)
        cells = jnp.concatenate(
            [
                lax.ppermute(tail, axis, [(i, (i + 1) % count) for i in range(ends)]),
                cells,
                lax.ppermute(head, axis, [((i + 1) % count, i) for i in range(ends)]),
            ],
            axis=dim,
        )
    return cells


def rotate(rows, positions):
    half_dim = rows.shape[-1] // 2
    inverse = THETA ** (-jnp.arange(half_dim, dtype=jnp.float32) / half_dim)
    angles = positions.astype(jnp.float32)[:, None] * inverse[None, :]
    cosine = jnp.cos(angles)[:, None, :]
    sine = jnp.sin(angles)[:, None, :]
    widened = rows.astype(jnp.float32)
    first_half = widened[..., :half_dim]
    second_half = widened[..., half_dim:]
    turned = jnp.concatenate(
        [first_half * cosine - second_half * sine, second_half * cosine + first_half * sine],
        axis=-1,
    )
    return turned.astype(jnp.bfloat16)


def to_blocks(rows):
    return rows.reshape(rows.shape[0] // BLOCK, BLOCK, rows.shape[1], rows.shape[2]).transpose(
        2, 0, 1, 3
    )


def from_blocks(blocks):
    return blocks.transpose(1, 2, 0, 3).reshape(
        blocks.shape[1] * blocks.shape[2], blocks.shape[0], blocks.shape[3]
    )


def blockwise(queries, key_rows, values, log_decay, include_diag):
    block_len = queries.shape[2]
    position = jnp.arange(block_len, dtype=jnp.float32)
    distance = position[:, None] - position[None, :]
    allowed = distance >= 0 if include_diag else distance > 0
    inside = jnp.where(
        allowed[None], jnp.exp(log_decay[:, None, None] * jnp.maximum(distance, 0.0)[None]), 0.0
    )
    query_wide = queries.astype(jnp.float32)
    key_wide = key_rows.astype(jnp.float32)
    value_wide = values.astype(jnp.float32)
    scores = (
        jnp.einsum("hnqd,hnkd->hnqk", query_wide, key_wide, precision=lax.Precision.HIGHEST)
        * inside[:, None]
    )
    inner_part = jnp.einsum("hnqk,hnkd->hnqd", scores, value_wide, precision=lax.Precision.HIGHEST)
    toward_end = jnp.exp(log_decay[:, None] * (block_len - 1.0 - position)[None])
    block_states = jnp.einsum(
        "hnkd,hnke->hnde",
        key_wide * toward_end[:, None, :, None],
        value_wide,
        precision=lax.Precision.HIGHEST,
    )
    block_decay = jnp.exp(log_decay * block_len)[:, None, None]

    def advance(state_now, block_state):
        return (block_decay * state_now + block_state, state_now)

    initial = jnp.zeros(
        (block_states.shape[0], block_states.shape[2], block_states.shape[3]), jnp.float32
    )
    final_state, earlier = lax.scan(advance, initial, jnp.moveaxis(block_states, 1, 0))
    earlier = jnp.moveaxis(earlier, 0, 1)
    from_start = jnp.exp(log_decay[:, None] * (position + 1.0)[None])
    cross_part = jnp.einsum(
        "hnqd,hnde->hnqe",
        query_wide * from_start[:, None, :, None],
        earlier,
        precision=lax.Precision.HIGHEST,
    )
    return (inner_part + cross_part, final_state)


def group_norm(retained, group_gain, group_bias, gate_rows):
    row_mean = jnp.mean(retained, axis=-1, keepdims=True)
    centered = retained - row_mean
    variance = jnp.mean(centered * centered, axis=-1, keepdims=True)
    scaled = (centered * lax.rsqrt(variance + EPS)).reshape(retained.shape[0], -1)
    scaled = scaled * group_gain[None, :] + group_bias[None, :]
    return (jax.nn.silu(gate_rows.astype(jnp.float32)) * scaled).astype(jnp.bfloat16)


def shards(
    hidden_states,
    norm_gain,
    query_weight,
    key_weight,
    value_weight,
    output_gate_weight,
    unit_input_weight,
    unit_gate_weight,
    decay_forward,
    decay_backward,
    group_gain,
    group_bias,
    depth_kernel,
    depth_bias,
    channel_gain,
    channel_bias,
    retention_out_weight,
    convolution_out_weight,
):
    row_total = hidden_states.shape[0]
    whole = lax.all_gather(hidden_states, "tp", axis=1, tiled=True)
    widened = whole.astype(jnp.float32)
    normed = (
        widened
        * lax.rsqrt(jnp.mean(widened * widened, axis=-1, keepdims=True) + EPS)
        * norm_gain[None, :]
    ).astype(jnp.bfloat16)
    slabs = (
        lax.all_gather(query_weight, "sp", axis=0, tiled=True),
        lax.all_gather(key_weight, "sp", axis=0, tiled=True),
        lax.all_gather(value_weight, "sp", axis=0, tiled=True),
        lax.all_gather(output_gate_weight, "sp", axis=0, tiled=True),
        lax.all_gather(unit_input_weight, "sp", axis=0, tiled=True),
        lax.all_gather(unit_gate_weight, "sp", axis=0, tiled=True),
    )
    summed = tuple((jnp.dot(normed, slab, preferred_element_type=jnp.float32) for slab in slabs))
    proj_q, proj_k, proj_v, proj_g, proj_a, proj_b = tuple(
        (part_sum.astype(jnp.bfloat16) for part_sum in summed)
    )
    head_count = proj_q.shape[1] // HEAD_DIM
    device = lax.axis_index("sp")
    positions = device * row_total + jnp.arange(row_total, dtype=jnp.int32)
    queries = rotate(proj_q.reshape(row_total, head_count, HEAD_DIM), positions)
    key_rows = rotate(proj_k.reshape(row_total, head_count, HEAD_DIM), positions)
    values = proj_v.reshape(row_total, head_count, HEAD_DIM)
    log_forward = jax.nn.log_sigmoid(decay_forward)
    log_backward = jax.nn.log_sigmoid(decay_backward)
    ahead_local, state_ahead = blockwise(
        to_blocks(queries), to_blocks(key_rows), to_blocks(values), log_forward, True
    )
    behind_local, state_behind = blockwise(
        to_blocks(queries[::-1]),
        to_blocks(key_rows[::-1]),
        to_blocks(values[::-1]),
        log_backward,
        False,
    )
    slabs = (
        lax.all_gather(state_ahead[None].astype(jnp.bfloat16), "sp", axis=0, tiled=True).astype(
            jnp.float32
        ),
        lax.all_gather(state_behind[None].astype(jnp.bfloat16), "sp", axis=0, tiled=True).astype(
            jnp.float32
        ),
    )
    source = jnp.arange(slabs[0].shape[0], dtype=jnp.int32)
    gap_ahead = device - 1 - source
    gap_behind = source - device - 1
    weight_ahead = jnp.where(
        gap_ahead[:, None] >= 0,
        jnp.exp(
            log_forward[None, :]
            * row_total
            * jnp.maximum(gap_ahead, 0).astype(jnp.float32)[:, None]
        ),
        0.0,
    )
    weight_behind = jnp.where(
        gap_behind[:, None] >= 0,
        jnp.exp(
            log_backward[None, :]
            * row_total
            * jnp.maximum(gap_behind, 0).astype(jnp.float32)[:, None]
        ),
        0.0,
    )
    enter_ahead = jnp.zeros_like(state_ahead) + jnp.einsum(
        "jh,jhde->hde", weight_ahead, slabs[0], precision=lax.Precision.HIGHEST
    )
    enter_behind = jnp.zeros_like(state_behind) + jnp.einsum(
        "jh,jhde->hde", weight_behind, slabs[1], precision=lax.Precision.HIGHEST
    )
    local_position = jnp.arange(row_total, dtype=jnp.float32)
    lift_ahead = jnp.exp(log_forward[None, :] * (local_position + 1.0)[:, None])
    lift_behind = jnp.exp(log_backward[None, :] * (row_total - local_position)[:, None])
    query_wide = queries.astype(jnp.float32)
    carried = jnp.einsum(
        "shd,hde->she",
        query_wide * lift_ahead[:, :, None],
        enter_ahead,
        precision=lax.Precision.HIGHEST,
    )
    carried = carried + jnp.einsum(
        "shd,hde->she",
        query_wide * lift_behind[:, :, None],
        enter_behind,
        precision=lax.Precision.HIGHEST,
    )
    retained = from_blocks(ahead_local) + from_blocks(behind_local)[::-1] + carried
    retention_rows = group_norm(retained, group_gain, group_bias, proj_g)
    unit = (proj_a.astype(jnp.float32) * jax.nn.sigmoid(proj_b.astype(jnp.float32))).astype(
        jnp.bfloat16
    )
    half_kernel = (KERNEL - 1) // 2
    padded = with_halo(unit, (("sp", 0),), half_kernel)
    filtered = jnp.broadcast_to(depth_bias[None, :], (row_total, unit.shape[1]))
    for offset in range(KERNEL):
        filtered = filtered + depth_kernel[offset][None, :] * padded[
            offset : offset + row_total
        ].astype(jnp.float32)
    row_sum, row_squares = lax.psum(
        (jnp.sum(filtered, axis=1), jnp.sum(filtered * filtered, axis=1)), "tp"
    )
    row_mean = (row_sum / CONV_WIDTH)[:, None]
    variance = (row_squares / CONV_WIDTH)[:, None] - row_mean * row_mean
    leveled = (filtered - row_mean) * lax.rsqrt(variance + EPS) * channel_gain[
        None, :
    ] + channel_bias[None, :]
    convolution_rows = jax.nn.silu(leveled).astype(jnp.bfloat16)
    retention_full, convolution_full = (
        lax.all_gather(retention_out_weight, "sp", axis=1, tiled=True),
        lax.all_gather(convolution_out_weight, "sp", axis=1, tiled=True),
    )
    return lax.psum_scatter(
        (
            jnp.dot(retention_rows, retention_full, preferred_element_type=jnp.float32)
            + jnp.dot(convolution_rows, convolution_full, preferred_element_type=jnp.float32)
        ).astype(jnp.bfloat16),
        "tp",
        scatter_dimension=0,
        tiled=True,
    )


def solution(mesh):
    placed = (
        P("sp", "tp"),
        P(),
        P("sp", "tp"),
        P("sp", "tp"),
        P("sp", "tp"),
        P("sp", "tp"),
        P("sp", "tp"),
        P("sp", "tp"),
        P("tp"),
        P("tp"),
        P("tp"),
        P("tp"),
        P(None, "tp"),
        P("tp"),
        P("tp"),
        P("tp"),
        P("tp", "sp"),
        P("tp", "sp"),
    )
    return jax.shard_map(
        shards, mesh=mesh, in_specs=placed, out_specs=P(("sp", "tp"), None), check_vma=False
    )
```

profile of v0, /device:TPU:0, one launch (start us, length us, event | category | flops | bytes accessed | tf_op | source)
XLA Modules:
  0.0 751.1 jit_solution(1209921822257919842)
XLA Ops:
  10.6 1.2 broadcast_multiply_fusion.2
  12.4 1.2 multiply_cosine_fusion
  13.6 20.6 %all-gather.14.cloned.1.call-done = bf16[256,4096]{1,0:T(8,128)(2,1)} async-done(((bf16[256,1024]{1,0:T(8,128)(2,1)}), bf16[256,4096]{1,0:T(8,128)(2,1)}) %all-gather.14.cloned.1.call-update) | async-done | bytes 2097168 | tf_op jit(solution)/shard_map/all_gather | solution.py:132
  34.2 2.1 fusion.1
  36.3 72.8 %all-gather.18.cloned.1.call-done = bf16[4096,512]{1,0:T(8,128)(2,1)} async-done(((bf16[512,512]{1,0:T(8,128)(2,1)}), bf16[4096,512]{1,0:T(8,128)(2,1)}) %all-gather.18.cloned.1.call-update) | async-done | bytes 4194320 | tf_op jit(solution)/shard_map/all_gather | solution.py:140
  109.2 4.1 fusion.15
  113.5 69.2 %all-gather.20.cloned.1.call-done = bf16[4096,512]{1,0:T(8,128)(2,1)} async-done(((bf16[512,512]{1,0:T(8,128)(2,1)}), bf16[4096,512]{1,0:T(8,128)(2,1)}) %all-gather.20.cloned.1.call-update) | async-done | bytes 4194320 | tf_op jit(solution)/shard_map/all_gather | solution.py:141
  182.7 3.5 fusion.14
  188.0 68.0 %all-gather.22.cloned.1.call-done = bf16[4096,512]{1,0:T(8,128)(2,1)} async-done(((bf16[512,512]{1,0:T(8,128)(2,1)}), bf16[4096,512]{1,0:T(8,128)(2,1)}) %all-gather.22.cloned.1.call-update) | async-done | bytes 4194320 | tf_op jit(solution)/shard_map/all_gather | solution.py:142
  256.0 4.1 convolution_convert_fusion.2
  267.1 0.8 exponential_select_fusion
  268.4 61.0 %all-gather.26.cloned.1.call-done = bf16[4096,512]{1,0:T(8,128)(2,1)} async-done(((bf16[512,512]{1,0:T(8,128)(2,1)}), bf16[4096,512]{1,0:T(8,128)(2,1)}) %all-gather.26.cloned.1.call-update) | async-done | bytes 4194320 | tf_op jit(solution)/shard_map/all_gather | solution.py:144
  329.4 4.9 fusion.13
  334.3 68.4 %all-gather.28.cloned.1.call-done = bf16[4096,512]{1,0:T(8,128)(2,1)} async-done(((bf16[512,512]{1,0:T(8,128)(2,1)}), bf16[4096,512]{1,0:T(8,128)(2,1)}) %all-gather.28.cloned.1.call-update) | async-done | bytes 4194320 | tf_op jit(solution)/shard_map/all_gather | solution.py:145
  402.7 4.3 fusion.12
  407.0 2.6 collective-permute-start
  409.6 1.5 collective-permute-start.1
  413.3 0.8 convolution_add_fusion.2
  415.6 3.7 fusion.97
  419.4 6.0 all-reduce
  425.4 18.2 %all-gather.34.cloned.1.call-done = bf16[32,128,128]{2,1,0:T(8,128)(2,1)} async-done(((bf16[4,128,128]{2,1,0:T(8,128)(2,1)}), bf16[32,128,128]{2,1,0:T(8,128)(2,1)}) %all-gather.34.cloned.1.call-update) | async-done | bytes 1048592 | tf_op jit(solution)/shard_map/all_gather | solution.py:173
  443.7 2.4 multiply_reduce_fusion
  446.1 38.7 %all-gather.32.cloned.1.call-done = bf16[32,128,128]{2,1,0:T(8,128)(2,1)} async-done(((bf16[4,128,128]{2,1,0:T(8,128)(2,1)}), bf16[32,128,128]{2,1,0:T(8,128)(2,1)}) %all-gather.32.cloned.1.call-update) | async-done | bytes 1048592 | tf_op jit(solution)/shard_map/all_gather | solution.py:170
  484.8 1.6 multiply_reduce_fusion.1
  486.4 0.8 fusion.17
  487.2 1.8 fusion.105
  489.4 69.1 %all-gather.16.cloned.1.call-done = bf16[4096,512]{1,0:T(8,128)(2,1)} async-done(((bf16[512,512]{1,0:T(8,128)(2,1)}), bf16[4096,512]{1,0:T(8,128)(2,1)}) %all-gather.16.cloned.1.call-update) | async-done | bytes 4194320 | tf_op jit(solution)/shard_map/all_gather | solution.py:143
  558.5 75.1 %all-gather.24.cloned.1.call-done = bf16[512,4096]{1,0:T(8,128)(2,1)} async-done(((bf16[512,512]{1,0:T(8,128)(2,1)}), bf16[512,4096]{1,0:T(8,128)(2,1)}) %all-gather.24.cloned.1.call-update) | async-done | bytes 4194320 | tf_op jit(solution)/shard_map/all_gather | solution.py:242
  633.6 8.0 %fusion.28 = f32[256,4096]{1,0:T(8,128)} fusion(bf16[512,4096]{1,0:T(8,128)(2,1)} %all-gather.24.cloned.1.call-done, f32[256,512]{1,0:T(8,128)S(1)} %copy.67, bf16[4096,512]{1,0:T(8,128)(2,1)} %all-gather.16.cloned.1.call-done, f32[512]{0:T(512)S(1)} %copy-done.43, f32[512]{0:T(512)S(1)} %copy-done.44, bf16[256,4096]{1,0:T(8,128)(2,1)S(1)} %copy-done.1, ...), kind=kOutput, calls=%fused_computation.89 | convolution fusion | flops 2152988672 | bytes 15225856 | tf_op jit(solution)/shard_map/dot_general | solution.py:247
  641.6 66.9 %all-gather.30.cloned.1.call-done = bf16[512,4096]{1,0:T(8,128)(2,1)} async-done(((bf16[512,512]{1,0:T(8,128)(2,1)}), bf16[512,4096]{1,0:T(8,128)(2,1)}) %all-gather.30.cloned.1.call-update) | async-done | bytes 4194320 | tf_op jit(solution)/shard_map/all_gather | solution.py:243
  708.5 6.2 fusion
  714.7 29.5 %reduce-scatter.2.cloned.1.call-done = bf16[64,4096]{1,0:T(8,128)(2,1)} async-done(((bf16[256,4096]{1,0:T(8,128)(2,1)}), bf16[64,4096]{1,0:T(8,128)(2,1)}) %reduce-scatter.2.cloned.1.call-update) | async-done | bytes 524304 | tf_op jit(solution)/shard_map/reduce_scatter | solution.py:245
  (185 shorter events, 17.9 us)
Async XLA Ops:
  6.5 102.6 %copy-start.38 = (f32[4096]{0:T(1024)S(1)}, f32[4096]{0:T(1024)}, u32[]{:S(2)}) copy-start(f32[4096]{0:T(1024)} %param.23) | copy-start | bytes 49156
  6.5 27.7 %all-gather.14.cloned.1.call-start = ((), (), s32[]{:S(2)}) async-start(), calls=%async_computation.1 | async-start | bytes 2621440 | tf_op jit(solution)/shard_map/all_gather | solution.py:132
  7.3 101.9 %all-gather.18.cloned.1.call-start = ((), (), s32[]{:S(2)}) async-start(), calls=%async_computation.3 | async-start | bytes 4718592 | tf_op jit(solution)/shard_map/all_gather | solution.py:140
  8.0 174.7 %all-gather.20.cloned.1.call-start = ((), (), s32[]{:S(2)}) async-start(), calls=%async_computation.4 | async-start | bytes 4718592 | tf_op jit(solution)/shard_map/all_gather | solution.py:141
  8.7 247.3 %all-gather.22.cloned.1.call-start = ((), (), s32[]{:S(2)}) async-start(), calls=%async_computation.5 | async-start | bytes 4718592 | tf_op jit(solution)/shard_map/all_gather | solution.py:142
  9.3 320.0 %all-gather.26.cloned.1.call-start = ((), (), s32[]{:S(2)}) async-start(), calls=%async_computation.7 | async-start | bytes 4718592 | tf_op jit(solution)/shard_map/all_gather | solution.py:144
  9.9 392.8 %all-gather.28.cloned.1.call-start = ((), (), s32[]{:S(2)}) async-start(), calls=%async_computation.8 | async-start | bytes 4718592 | tf_op jit(solution)/shard_map/all_gather | solution.py:145
  10.5 433.2 %all-gather.34.cloned.1.call-start = ((), (), s32[]{:S(2)}) async-start(), calls=%async_computation.12 | async-start | bytes 1179648 | tf_op jit(solution)/shard_map/all_gather | solution.py:173
  11.8 24.5 %copy-start.27 = (f32[4]{0:T(128)}, f32[4]{0:T(128)S(1)}, u32[]{:S(2)}) copy-start(f32[4]{0:T(128)S(1)} %get-tuple-element.208) | copy-start | bytes 52
  36.3 72.8 %copy-start.33 = (f32[256]{0:T(256)}, f32[256]{0:T(256)S(1)}, u32[]{:S(2)}) copy-start(f32[256]{0:T(256)S(1)} %add_rsqrt_fusion.2) | copy-start | bytes 3076
  36.3 146.4 %copy-start = (bf16[256,4096]{1,0:T(8,128)(2,1)S(1)}, bf16[256,4096]{1,0:T(8,128)(2,1)}, u32[]{:S(2)}) copy-start(bf16[256,4096]{1,0:T(8,128)(2,1)} %all-gather.14.cloned.1.call-done) | copy-start | bytes 6291460
  186.4 69.6 %copy-start.34 = (f32[256]{0:T(256)S(1)}, f32[256]{0:T(256)}, u32[]{:S(2)}) copy-start(f32[256]{0:T(256)} %copy-done.33) | copy-start | bytes 3076
  186.4 69.6 %copy-start.39 = (f32[4096]{0:T(1024)S(1)}, f32[4096]{0:T(1024)}, u32[]{:S(2)}) copy-start(f32[4096]{0:T(1024)} %param.23) | copy-start | bytes 49156
  261.9 222.9 %all-gather.32.cloned.1.call-start = ((), (), s32[]{:S(2)}) async-start(), calls=%async_computation.11 | async-start | bytes 1179648 | tf_op jit(solution)/shard_map/all_gather | solution.py:170
  263.2 66.2 %copy-start.35 = (f32[256]{0:T(256)S(1)}, f32[256]{0:T(256)}, u32[]{:S(2)}) copy-start(f32[256]{0:T(256)} %copy-done.33) | copy-start | bytes 3076
  263.2 66.2 %copy-start.40 = (f32[4096]{0:T(1024)S(1)}, f32[4096]{0:T(1024)}, u32[]{:S(2)}) copy-start(f32[4096]{0:T(1024)} %param.23) | copy-start | bytes 49156
  263.9 294.6 %all-gather.16.cloned.1.call-start = ((), (), s32[]{:S(2)}) async-start(), calls=%async_computation.2 | async-start | bytes 4718592 | tf_op jit(solution)/shard_map/all_gather | solution.py:143
  264.6 369.0 %all-gather.24.cloned.1.call-start = ((), (), s32[]{:S(2)}) async-start(), calls=%async_computation.6 | async-start | bytes 4718592 | tf_op jit(solution)/shard_map/all_gather | solution.py:242
  265.2 443.3 %all-gather.30.cloned.1.call-start = ((), (), s32[]{:S(2)}) async-start(), calls=%async_computation.9 | async-start | bytes 4718592 | tf_op jit(solution)/shard_map/all_gather | solution.py:243
  265.9 478.3 %reduce-scatter.2.cloned.1.call-start = ((), (), s32[]{:S(2)}) async-start(), calls=%async_computation.10 | async-start | bytes 2621440 | tf_op jit(solution)/shard_map/reduce_scatter | solution.py:245
  268.4 134.3 %copy-start.36 = (f32[256]{0:T(256)S(1)}, f32[256]{0:T(256)}, u32[]{:S(2)}) copy-start(f32[256]{0:T(256)} %copy-done.33) | copy-start | bytes 3076
  268.4 134.3 %copy-start.41 = (f32[4096]{0:T(1024)S(1)}, f32[4096]{0:T(1024)}, u32[]{:S(2)}) copy-start(f32[4096]{0:T(1024)} %param.23) | copy-start | bytes 49156
  407.0 8.2 %collective-permute-start = (bf16[15,512]{1,0:T(8,128)(2,1)S(1)}, bf16[15,512]{1,0:T(8,128)(2,1)S(1)}, u32[]{:S(2)}, u32[]{:S(2)}) collective-permute-start(bf16[15,512]{1,0:T(8,128)(2,1)S(1)} %get-tuple-element.158), channel_id=1, source_target_pairs={{0,4},{4,8},{8,12},{12,16},{16,20},{20,24},{24,28},{1,5},{5,9},{9,... | collective-permute-start | bytes 46088 | tf_op jit(solution)/shard_map/ppermute | solution.py:22
  409.6 5.9 collective-permute-start.1
  443.7 189.9 %copy-start.1 = (bf16[256,4096]{1,0:T(8,128)(2,1)S(1)}, bf16[256,4096]{1,0:T(8,128)(2,1)}, u32[]{:S(2)}) copy-start(bf16[256,4096]{1,0:T(8,128)(2,1)} %all-gather.14.cloned.1.call-done) | copy-start | bytes 6291460
  443.7 189.9 %copy-start.37 = (f32[256]{0:T(256)S(1)}, f32[256]{0:T(256)}, u32[]{:S(2)}) copy-start(f32[256]{0:T(256)} %copy-done.33) | copy-start | bytes 3076
  443.7 189.9 %copy-start.42 = (f32[4096]{0:T(1024)S(1)}, f32[4096]{0:T(1024)}, u32[]{:S(2)}) copy-start(f32[4096]{0:T(1024)} %param.23) | copy-start | bytes 49156
  443.7 189.9 %copy-start.43 = (f32[512]{0:T(512)S(1)}, f32[512]{0:T(512)}, u32[]{:S(2)}) copy-start(f32[512]{0:T(512)} %param.33) | copy-start | bytes 6148
  443.7 189.9 %copy-start.44 = (f32[512]{0:T(512)S(1)}, f32[512]{0:T(512)}, u32[]{:S(2)}) copy-start(f32[512]{0:T(512)} %param.32) | copy-start | bytes 6148
  489.3 219.1 %copy-start.4 = (f32[256,512]{1,0:T(8,128)S(1)}, f32[256,512]{1,0:T(8,128)}, u32[]{:S(2)}) copy-start(f32[256,512]{1,0:T(8,128)} %get-tuple-element.145) | copy-start | bytes 1572868
  489.3 219.1 %copy-start.7 = (f32[512]{0:T(512)S(1)}, f32[512]{0:T(512)}, u32[]{:S(2)}) copy-start(f32[512]{0:T(512)} %param.37) | copy-start | bytes 6148
  489.4 219.1 %copy-start.8 = (f32[512]{0:T(512)S(1)}, f32[512]{0:T(512)}, u32[]{:S(2)}) copy-start(f32[512]{0:T(512)} %param.36) | copy-start | bytes 6148
  (27 other events, 106.0 us)
Sparse Core Ops, SparseCore 0:
  8.9 25.2 all-gather.13
  36.3 72.7 all-gather.17
  111.3 71.3 all-gather.19
  184.7 71.3 all-gather.21
  258.0 71.3 all-gather.25
  331.3 71.3 all-gather.27
  404.8 38.8 all-gather.33
  445.8 38.9 all-gather.31
  487.0 71.4 all-gather.15
  560.4 73.1 all-gather.23
  635.6 72.8 all-gather.29
  714.8 29.3 reduce-scatter.1
where the time goes:
time: 751 us
  waiting for transfers between devices  663 us (88%)
  matrix products  41.3 us (5%)
  other arithmetic  16.6 us (2%)
  between operations  14.5 us (2%)
    all_gather x1, waiting for transfers between devices, shards(): lax.all_gather(retention_out_weight, 'sp', axis=1, tiled=True)  75.1 us
    all_gather x1, waiting for transfers between devices, shards(): lax.all_gather(query_weight, 'sp', axis=0, tiled=True)  72.8 us
    all_gather x1, waiting for transfers between devices, shards(): lax.all_gather(key_weight, 'sp', axis=0, tiled=True)  69.2 us
    all_gather x1, waiting for transfers between devices, shards(): lax.all_gather(output_gate_weight, 'sp', axis=0, tiled=True)  69.1 us
    all_gather x1, waiting for transfers between devices, shards(): lax.all_gather(unit_gate_weight, 'sp', axis=0, tiled=True)  68.4 us
    all_gather x1, waiting for transfers between devices, shards(): lax.all_gather(value_weight, 'sp', axis=0, tiled=True)  68 us
    all_gather x1, waiting for transfers between devices, shards(): lax.all_gather(convolution_out_weight, 'sp', axis=1, tiled=True)  66.9 us
    all_gather x1, waiting for transfers between devices, shards(): lax.all_gather(unit_input_weight, 'sp', axis=0, tiled=True)  61 us
  transfers between devices with their start and end apart: 14, of which 13 were waited for; matrix products, arithmetic and copies ran while one was open for 7% of the time, Pallas kernels for 0%

commit v1 on v0

--- a/solution.py
+++ b/solution.py
@@ -240,7 +240,7 @@
     convolution_rows = jax.nn.silu(leveled).astype(jnp.bfloat16)
     retention_full, convolution_full = (
         lax.all_gather(retention_out_weight, "sp", axis=1, tiled=True),
-        lax.all_gather(convolution_out_weight, "sp", axis=1, tiled=True),
+        jnp.concatenate(lax.all_gather(convolution_out_weight, "sp"), axis=1),
     )
     return lax.psum_scatter(
         (

time: 751 us -> 759 us (1.011)
  transfers between devices with their start and end apart: 14 -> 14, of which waited for: 13 -> 12; matrix products, arithmetic and copies ran while one was open for 7% -> 7% of each run, Pallas kernels for 0% -> 0%
where the time goes in v1:
time: 759 us; the launch traced here: 758 us
  waiting for transfers between devices  667 us (88%)
  matrix products  42.2 us (6%)
  between operations  14.3 us (2%)
  other arithmetic  13.5 us (2%)
  local copies, waits for them, and re-layouts  10.7 us (1%)
    all_gather x1, waiting for transfers between devices, shards(): lax.all_gather(retention_out_weight, 'sp', axis=1, tiled=True)  75.3 us
    all_gather x1, waiting for transfers between devices, shards(): lax.all_gather(query_weight, 'sp', axis=0, tiled=True)  72.8 us
    all_gather x1, waiting for transfers between devices, shards(): lax.all_gather(output_gate_weight, 'sp', axis=0, tiled=True)  69.9 us
    all_gather x1, waiting for transfers between devices, shards(): lax.all_gather(key_weight, 'sp', axis=0, tiled=True)  69.2 us
    all_gather x1, waiting for transfers between devices, shards(): lax.all_gather(unit_gate_weight, 'sp', axis=0, tiled=True)  68.4 us
    all_gather x1, waiting for transfers between devices, shards(): lax.all_gather(value_weight, 'sp', axis=0, tiled=True)  67.7 us
    all_gather x1, waiting for transfers between devices, shards(): lax.all_gather(unit_input_weight, 'sp', axis=0, tiled=True)  62.2 us
    all_gather x1, waiting for transfers between devices, shards(): lax.all_gather(convolution_out_weight, 'sp')  60.9 us
  transfers between devices with their start and end apart: 14, of which 12 were waited for; matrix products, arithmetic and copies ran while one was open for 7% of the time, Pallas kernels for 0%

profile of v1, /device:TPU:0, one launch (start us, length us, event | category | flops | bytes accessed | tf_op | source)
XLA Modules:
  0.0 758.4 jit_solution(10775580775504107831)
XLA Ops:
  13.3 21.0 %all-gather.15.cloned.1.call-done = bf16[256,4096]{1,0:T(8,128)(2,1)} async-done(((bf16[256,1024]{1,0:T(8,128)(2,1)}), bf16[256,4096]{1,0:T(8,128)(2,1)}) %all-gather.15.cloned.1.call-update) | async-done | bytes 2097168 | tf_op jit(solution)/shard_map/all_gather | solution.py:132
  34.2 2.1 fusion.1
  36.3 72.8 %all-gather.19.cloned.1.call-done = bf16[4096,512]{1,0:T(8,128)(2,1)} async-done(((bf16[512,512]{1,0:T(8,128)(2,1)}), bf16[4096,512]{1,0:T(8,128)(2,1)}) %all-gather.19.cloned.1.call-update) | async-done | bytes 4194320 | tf_op jit(solution)/shard_map/all_gather | solution.py:140
  109.2 4.1 fusion.15
  113.5 69.2 %all-gather.21.cloned.1.call-done = bf16[4096,512]{1,0:T(8,128)(2,1)} async-done(((bf16[512,512]{1,0:T(8,128)(2,1)}), bf16[4096,512]{1,0:T(8,128)(2,1)}) %all-gather.21.cloned.1.call-update) | async-done | bytes 4194320 | tf_op jit(solution)/shard_map/all_gather | solution.py:141
  182.7 4.1 fusion.14
  188.4 67.7 %all-gather.23.cloned.1.call-done = bf16[4096,512]{1,0:T(8,128)(2,1)} async-done(((bf16[512,512]{1,0:T(8,128)(2,1)}), bf16[4096,512]{1,0:T(8,128)(2,1)}) %all-gather.23.cloned.1.call-update) | async-done | bytes 4194320 | tf_op jit(solution)/shard_map/all_gather | solution.py:142
  256.0 4.1 convolution_convert_fusion.2
  262.2 0.8 convolution_bitcast_fusion.1
  267.2 62.2 %all-gather.27.cloned.1.call-done = bf16[4096,512]{1,0:T(8,128)(2,1)} async-done(((bf16[512,512]{1,0:T(8,128)(2,1)}), bf16[4096,512]{1,0:T(8,128)(2,1)}) %all-gather.27.cloned.1.call-update) | async-done | bytes 4194320 | tf_op jit(solution)/shard_map/all_gather | solution.py:144
  329.4 4.9 fusion.13
  334.3 68.4 %all-gather.29.cloned.1.call-done = bf16[4096,512]{1,0:T(8,128)(2,1)} async-done(((bf16[512,512]{1,0:T(8,128)(2,1)}), bf16[4096,512]{1,0:T(8,128)(2,1)}) %all-gather.29.cloned.1.call-update) | async-done | bytes 4194320 | tf_op jit(solution)/shard_map/all_gather | solution.py:145
  402.7 4.3 fusion.12
  407.1 2.6 collective-permute-start
  409.7 1.5 collective-permute-start.1
  413.4 0.8 convolution_add_fusion.2
  414.4 0.7 rev.15
  415.3 60.9 %all-gather.35.cloned.1.call-done = bf16[4096,512]{1,0:T(8,128)(2,1)} async-done(((bf16[512,512]{1,0:T(8,128)(2,1)}), bf16[4096,512]{1,0:T(8,128)(2,1)}) %all-gather.35.cloned.1.call-update) | async-done | bytes 4194320 | tf_op jit(solution)/shard_map/all_gather | solution.py:243
  476.4 6.5 copy.84
  483.0 3.2 fusion.96
  486.2 5.9 all-reduce
  492.1 25.1 %all-gather.33.cloned.1.call-done = bf16[32,128,128]{2,1,0:T(8,128)(2,1)} async-done(((bf16[4,128,128]{2,1,0:T(8,128)(2,1)}), bf16[32,128,128]{2,1,0:T(8,128)(2,1)}) %all-gather.33.cloned.1.call-update) | async-done | bytes 1048592 | tf_op jit(solution)/shard_map/all_gather | solution.py:173
  517.2 1.6 multiply_reduce_fusion
  518.8 39.6 %all-gather.31.cloned.1.call-done = bf16[32,128,128]{2,1,0:T(8,128)(2,1)} async-done(((bf16[4,128,128]{2,1,0:T(8,128)(2,1)}), bf16[32,128,128]{2,1,0:T(8,128)(2,1)}) %all-gather.31.cloned.1.call-update) | async-done | bytes 1048592 | tf_op jit(solution)/shard_map/all_gather | solution.py:170
  558.3 1.6 multiply_reduce_fusion.1
  559.9 0.8 fusion.17
  560.7 0.8 fusion.104
  561.9 69.9 %all-gather.17.cloned.1.call-done = bf16[4096,512]{1,0:T(8,128)(2,1)} async-done(((bf16[512,512]{1,0:T(8,128)(2,1)}), bf16[4096,512]{1,0:T(8,128)(2,1)}) %all-gather.17.cloned.1.call-update) | async-done | bytes 4194320 | tf_op jit(solution)/shard_map/all_gather | solution.py:143
  631.9 75.3 %all-gather.25.cloned.1.call-done = bf16[512,4096]{1,0:T(8,128)(2,1)} async-done(((bf16[512,512]{1,0:T(8,128)(2,1)}), bf16[512,4096]{1,0:T(8,128)(2,1)}) %all-gather.25.cloned.1.call-update) | async-done | bytes 4194320 | tf_op jit(solution)/shard_map/all_gather | solution.py:242
  707.1 8.7 %fusion.28 = f32[256,4096]{1,0:T(8,128)} fusion(bf16[512,4096]{1,0:T(8,128)(2,1)} %all-gather.25.cloned.1.call-done, f32[256,512]{1,0:T(8,128)S(1)} %copy.105, bf16[4096,512]{1,0:T(8,128)(2,1)} %all-gather.17.cloned.1.call-done, f32[512]{0:T(512)S(1)} %copy-done.29, f32[512]{0:T(512)S(1)} %copy-done.30, ...), kind=kOutput, calls=%fused_computation.89 | convolution fusion | flops 2152988672 | bytes 15225856 | tf_op jit(solution)/shard_map/dot_general | solution.py:247
  715.8 6.2 fusion
  722.0 29.5 %reduce-scatter.2.cloned.1.call-done = bf16[64,4096]{1,0:T(8,128)(2,1)} async-done(((bf16[256,4096]{1,0:T(8,128)(2,1)}), bf16[64,4096]{1,0:T(8,128)(2,1)}) %reduce-scatter.2.cloned.1.call-update) | async-done | bytes 524304 | tf_op jit(solution)/shard_map/reduce_scatter | solution.py:245
  (156 shorter events, 17.8 us)
Async XLA Ops:
  6.5 102.6 %copy-start.27 = (f32[4096]{0:T(1024)S(1)}, f32[4096]{0:T(1024)}, u32[]{:S(2)}) copy-start(f32[4096]{0:T(1024)} %param.23) | copy-start | bytes 49156
  6.5 27.7 %all-gather.15.cloned.1.call-start = ((), (), s32[]{:S(2)}) async-start(), calls=%async_computation.1 | async-start | bytes 2621440 | tf_op jit(solution)/shard_map/all_gather | solution.py:132
  7.3 101.9 %all-gather.19.cloned.1.call-start = ((), (), s32[]{:S(2)}) async-start(), calls=%async_computation.3 | async-start | bytes 4718592 | tf_op jit(solution)/shard_map/all_gather | solution.py:140
  8.0 174.7 %all-gather.21.cloned.1.call-start = ((), (), s32[]{:S(2)}) async-start(), calls=%async_computation.4 | async-start | bytes 4718592 | tf_op jit(solution)/shard_map/all_gather | solution.py:141
  8.7 247.3 %all-gather.23.cloned.1.call-start = ((), (), s32[]{:S(2)}) async-start(), calls=%async_computation.5 | async-start | bytes 4718592 | tf_op jit(solution)/shard_map/all_gather | solution.py:142
  9.3 320.1 %all-gather.27.cloned.1.call-start = ((), (), s32[]{:S(2)}) async-start(), calls=%async_computation.7 | async-start | bytes 4718592 | tf_op jit(solution)/shard_map/all_gather | solution.py:144
  9.9 392.8 %all-gather.29.cloned.1.call-start = ((), (), s32[]{:S(2)}) async-start(), calls=%async_computation.8 | async-start | bytes 4718592 | tf_op jit(solution)/shard_map/all_gather | solution.py:145
  10.5 465.7 %all-gather.35.cloned.1.call-start = ((), (), s32[]{:S(2)}) async-start(), calls=%async_computation.12 | async-start | bytes 4718592 | tf_op jit(solution)/shard_map/all_gather | solution.py:243
  11.2 506.0 %all-gather.33.cloned.1.call-start = ((), (), s32[]{:S(2)}) async-start(), calls=%async_computation.11 | async-start | bytes 1179648 | tf_op jit(solution)/shard_map/all_gather | solution.py:173
  36.3 366.4 %copy-start.25 = (f32[256]{0:T(256)}, f32[256]{0:T(256)S(1)}, u32[]{:S(2)}) copy-start(f32[256]{0:T(256)S(1)} %add_rsqrt_fusion.2) | copy-start | bytes 3076
  262.0 296.3 %all-gather.31.cloned.1.call-start = ((), (), s32[]{:S(2)}) async-start(), calls=%async_computation.10 | async-start | bytes 1179648 | tf_op jit(solution)/shard_map/all_gather | solution.py:170
  264.0 367.8 %all-gather.17.cloned.1.call-start = ((), (), s32[]{:S(2)}) async-start(), calls=%async_computation.2 | async-start | bytes 4718592 | tf_op jit(solution)/shard_map/all_gather | solution.py:143
  264.6 442.5 %all-gather.25.cloned.1.call-start = ((), (), s32[]{:S(2)}) async-start(), calls=%async_computation.6 | async-start | bytes 4718592 | tf_op jit(solution)/shard_map/all_gather | solution.py:242
  265.4 486.2 %reduce-scatter.2.cloned.1.call-start = ((), (), s32[]{:S(2)}) async-start(), calls=%async_computation.9 | async-start | bytes 2621440 | tf_op jit(solution)/shard_map/reduce_scatter | solution.py:245
  407.0 7.1 copy-start.2
  407.1 75.8 %collective-permute-start = (bf16[15,512]{1,0:T(8,128)(2,1)S(1)}, bf16[15,512]{1,0:T(8,128)(2,1)S(1)}, u32[]{:S(2)}, u32[]{:S(2)}) collective-permute-start(bf16[15,512]{1,0:T(8,128)(2,1)S(1)} %get-tuple-element.178), channel_id=1, source_target_pairs={{0,4},{4,8},{8,12},{12,16},{16,20},{20,24},{24,28},{1,5},{5,9},{9,... | collective-permute-start | bytes 46088 | tf_op jit(solution)/shard_map/ppermute | solution.py:22
  409.7 73.2 %collective-permute-start.1 = (bf16[15,512]{1,0:T(8,128)(2,1)S(1)}, bf16[15,512]{1,0:T(8,128)(2,1)S(1)}, u32[]{:S(2)}, u32[]{:S(2)}) collective-permute-start(bf16[15,512]{1,0:T(8,128)(2,1)S(1)} %get-tuple-element.179), channel_id=1, source_target_pairs={{4,0},{8,4},{12,8},{16,12},{20,16},{24,20},{28,24},{5,1},{9,5},{13... | collective-permute-start | bytes 46088 | tf_op jit(solution)/shard_map/ppermute | solution.py:24
  476.2 6.7 copy-start.9
  476.3 6.7 copy-start.10
  476.3 6.7 copy-start.11
  476.3 6.7 copy-start.12
  476.3 6.7 copy-start.13
  476.3 6.7 copy-start.14
  476.3 6.7 copy-start.15
  476.3 6.7 copy-start.16
  476.3 6.7 copy-start.17
  517.2 189.9 %copy-start.26 = (f32[256]{0:T(256)S(1)}, f32[256]{0:T(256)}, u32[]{:S(2)}) copy-start(f32[256]{0:T(256)} %copy-done.25) | copy-start | bytes 3076
  517.2 189.9 %copy-start.28 = (f32[4096]{0:T(1024)S(1)}, f32[4096]{0:T(1024)}, u32[]{:S(2)}) copy-start(f32[4096]{0:T(1024)} %param.23) | copy-start | bytes 49156
  517.2 189.9 %copy-start.29 = (f32[512]{0:T(512)S(1)}, f32[512]{0:T(512)}, u32[]{:S(2)}) copy-start(f32[512]{0:T(512)} %param.33) | copy-start | bytes 6148
  517.2 189.9 %copy-start.30 = (f32[512]{0:T(512)S(1)}, f32[512]{0:T(512)}, u32[]{:S(2)}) copy-start(f32[512]{0:T(512)} %param.32) | copy-start | bytes 6148
  561.9 153.9 %copy-start.23 = (f32[512]{0:T(512)S(1)}, f32[512]{0:T(512)}, u32[]{:S(2)}) copy-start(f32[512]{0:T(512)} %param.37) | copy-start | bytes 6148
  561.9 153.9 %copy-start.24 = (f32[512]{0:T(512)S(1)}, f32[512]{0:T(512)}, u32[]{:S(2)}) copy-start(f32[512]{0:T(512)} %param.36) | copy-start | bytes 6148
  (13 other events, 74.7 us)
Sparse Core Ops, SparseCore 0:
  8.9 25.2 all-gather.14
  36.3 72.7 all-gather.18
  111.3 71.3 all-gather.20
  184.7 71.3 all-gather.22
  258.0 71.3 all-gather.26
  331.4 71.3 all-gather.28
  404.9 71.3 all-gather.34
  478.4 38.7 all-gather.32
  519.3 38.9 all-gather.30
  560.3 71.4 all-gather.16
  633.9 73.1 all-gather.24
  722.2 29.3 reduce-scatter.1
